TPU v7x, 32 devices: a whole 2x2x4 slice. The times are simulated.
32 devices in a mesh: kv: 4 (over y, x), tp: 8 (over z, core).
Axes of the slice: x: 2, y: 2, z: 4, core: 2. Of those that a mesh axis runs over, the one named last changes fastest.
Arguments:
- stream: bfloat16 [32, 4096], P(None, ('kv', 'tp')), may hold values from -18 to 18
- mixer_gain: float32 [4096], replicated, may hold values from 0.1 to 1.9
- query_weight: bfloat16 [4096, 1024], P(None, 'tp'), may hold values from -0.09375 to 0.09375
- key_weight: bfloat16 [4096, 1024], P(None, 'tp'), may hold values from -0.09375 to 0.09375
- value_weight: bfloat16 [4096, 1024], P(None, 'tp'), may hold values from -0.09375 to 0.09375
- forget_weight: bfloat16 [4096, 16], replicated, may hold values from -0.09375 to 0.09375
- forget_bias: float32 [16], replicated, may hold values from -4 to -2
- key_cache: bfloat16 [32, 16, 4096, 64], P(None, 'tp', 'kv'), may hold values from -512 to 512, as said below
- value_cache: bfloat16 [32, 16, 4096, 64], P(None, 'tp', 'kv'), may hold values from -12 to 12
- past_decay: float32 [32, 16, 4096], P(None, 'tp', 'kv'), may hold values from -4096 to 0, as said below
- out_weight: bfloat16 [1024, 4096], P('tp', 'kv'), may hold values from -0.75 to 0.75
- channel_gain: float32 [4096], replicated, may hold values from 0.1 to 1.9
- up_weight: bfloat16 [4096, 16384], P('kv', 'tp'), may hold values from -0.09375 to 0.09375
- down_weight: bfloat16 [16384, 4096], P('tp', 'kv'), may hold values from -0.0625 to 0.0625
Outputs:
- updated: bfloat16 [32, 4096], P(None, ('kv', 'tp'))
Inputs may be any that keep to these rules, and one draw needn't show every extreme that they name: `key_cache`: keys of order one; some cached keys may be much larger. `past_decay`: never falling along the positions of a sequence and head, zero at the last cached position.
All inputs are finite; a program needn't handle non-finite values.
Results may differ from a plain program's by a relative error of at most 0.014.
The roundings to bfloat16 on the way count: a program that leaves them out, or rounds other values in their place, can miss the bound.
Values may be sent and summed in bfloat16 or wider, within the bound.
No kernel may reach another device: no remote copies, remote signals or barrier semaphores. Data moves between devices by JAX's collectives and lax.ppermute only.
A program may use at most 64 MiB of HBM per device.

v0:
```python
import jax
import jax.numpy as jnp
from jax import lax
from jax.sharding import PartitionSpec as P

D = 4096
EPS = 1e-06


def combined_all(part, axis, combine):
    gathered = jax.tree.map(lambda a: lax.all_gather(a, axis), part)

    def take(source):
        return jax.tree.map(lambda a: lax.dynamic_index_in_dim(a, source, 0, False), gathered)

    return lax.fori_loop(
        1, lax.axis_size(axis), lambda source, state: combine(state, take(source)), take(0)
    )


def rms_scale(values, gain):
    widened = values.astype(jnp.float32)
    inverse = lax.rsqrt(jnp.mean(widened * widened, axis=-1, keepdims=True) + EPS)
    return (widened * inverse * gain).astype(jnp.bfloat16)


def merge_parts(earlier, later):
    top_one, total_one, sums_one = earlier
    top_two, total_two, sums_two = later
    highest = jnp.maximum(top_one, top_two)
    factor_one = jnp.exp(top_one - highest)
    factor_two = jnp.exp(top_two - highest)
    return (
        highest,
        total_one * factor_one + total_two * factor_two,
        sums_one * factor_one[..., None] + sums_two * factor_two[..., None],
    )


def squared_relu(values):
    return jnp.square(jax.nn.relu(values)).astype(jnp.bfloat16)


def row_squares(values):
    widened = values.astype(jnp.float32)
    return jnp.sum(widened * widened, axis=1)


def shards(
    stream,
    mixer_gain,
    query_weight,
    key_weight,
    value_weight,
    forget_weight,
    forget_bias,
    key_cache,
    value_cache,
    past_decay,
    out_weight,
    channel_gain,
    up_weight,
    down_weight,
):
    batch_rows = stream.shape[0]
    local_heads = key_cache.shape[1]
    head_size = key_cache.shape[3]
    scale_factor = float(head_size) ** (-0.5)
    gathered = lax.all_gather(stream, ("kv", "tp"), axis=1, tiled=True)
    normed = rms_scale(gathered, mixer_gain)
    queries = jnp.dot(normed, query_weight, preferred_element_type=jnp.float32).astype(jnp.bfloat16)
    keys_new = jnp.dot(normed, key_weight, preferred_element_type=jnp.float32).astype(jnp.bfloat16)
    values_new = jnp.dot(normed, value_weight, preferred_element_type=jnp.float32).astype(
        jnp.bfloat16
    )
    forget_all = jax.nn.log_sigmoid(
        jnp.dot(normed, forget_weight, preferred_element_type=jnp.float32) + forget_bias
    )
    forget = lax.dynamic_slice_in_dim(
        forget_all, lax.axis_index("tp") * local_heads, local_heads, 1
    )
    query_heads = queries.reshape(batch_rows, local_heads, head_size)
    scores = (
        jnp.einsum("bhd,bhpd->bhp", query_heads, key_cache, preferred_element_type=jnp.float32)
        * scale_factor
        + forget[..., None]
        + past_decay
    )
    highest = jnp.max(scores, axis=-1)
    weights = jnp.exp(scores - highest[..., None]).astype(jnp.bfloat16)
    totals = jnp.sum(weights.astype(jnp.float32), axis=-1)
    sums = jnp.einsum("bhp,bhpd->bhd", weights, value_cache, preferred_element_type=jnp.float32)
    highest, totals, sums = combined_all((highest, totals, sums), "kv", merge_parts)
    key_heads = keys_new.reshape(batch_rows, local_heads, head_size).astype(jnp.float32)
    value_heads = values_new.reshape(batch_rows, local_heads, head_size).astype(jnp.float32)
    own = jnp.sum(query_heads.astype(jnp.float32) * key_heads, axis=-1) * scale_factor
    peak = jnp.maximum(highest, own)
    cache_factor = jnp.exp(highest - peak)
    own_factor = jnp.exp(own - peak)
    numer = sums * cache_factor[..., None] + value_heads * own_factor[..., None]
    denom = totals * cache_factor + own_factor
    attention = (
        (numer / denom[..., None]).astype(jnp.bfloat16).reshape(batch_rows, local_heads * head_size)
    )
    partial_value = jnp.dot(attention, out_weight, preferred_element_type=jnp.float32)
    piece_width = stream.shape[1]
    block_width = partial_value.shape[1]
    block_sum = lax.psum(partial_value, "tp")
    own_block = lax.dynamic_slice_in_dim(
        gathered, lax.axis_index("kv") * block_width, block_width, 1
    )
    middle_block = (own_block.astype(jnp.float32) + block_sum).astype(jnp.bfloat16)
    squares = lax.psum(row_squares(middle_block), "kv")
    middle_piece = lax.dynamic_slice_in_dim(
        middle_block, lax.axis_index("tp") * piece_width, piece_width, 1
    )
    inverse = lax.rsqrt(squares / D + EPS)
    gain_block = lax.dynamic_slice_in_dim(
        channel_gain, lax.axis_index("kv") * block_width, block_width, 0
    )
    mixed_block = (
        middle_block.astype(jnp.float32) * inverse[:, None] * gain_block[None, :]
    ).astype(jnp.bfloat16)
    up_partial = jnp.dot(mixed_block, up_weight, preferred_element_type=jnp.float32)
    hidden = squared_relu(lax.psum(up_partial, "kv"))
    down_partial = jnp.dot(hidden, down_weight, preferred_element_type=jnp.float32)
    reduced = lax.psum_scatter(down_partial, "tp", scatter_dimension=1, tiled=True)
    return (middle_piece.astype(jnp.float32) + reduced).astype(jnp.bfloat16)


def solution(mesh):
    return jax.shard_map(
        shards,
        mesh=mesh,
        in_specs=(
            P(None, ("kv", "tp")),
            P(),
            P(None, "tp"),
            P(None, "tp"),
            P(None, "tp"),
            P(),
            P(),
            P(None, "tp", "kv", None),
            P(None, "tp", "kv", None),
            P(None, "tp", "kv"),
            P("tp", "kv"),
            P(),
            P("kv", "tp"),
            P("tp", "kv"),
        ),
        out_specs=P(None, ("kv", "tp")),
        check_vma=False,
    )
```

profile of v0, /device:TPU:0, one launch (start us, length us, event | category | flops | bytes accessed | tf_op | source)
XLA Modules:
  0.0 247.9 jit_solution(13276194251928122677)
XLA Ops:
  6.5 44.6 %all_gather.21 = bf16[32,4096]{1,0:T(8,128)(2,1)S(1)} all-gather(bf16[32,128]{1,0:T(8,128)(2,1)} %param.16), channel_id=1, replica_groups=mesh['kv'=4,'tp'=8] {'kv','tp'}, dimensions={1}, use_global_device_ids=true | all-gather | bytes 270336 | tf_op jit(solution)/shard_map/all_gather | solution.py:69
  51.2 0.2 fusion.6
  51.4 1.0 convolution_convert_fusion.2
  52.6 1.2 fusion.40
  53.9 4.6 %fusion.41 = f32[32,2,1,1024]{3,2,1,0:T(1,128)S(1)} fusion(bf16[32,2,64,1]{2,3,1,0:T(2,128)(2,1)S(1)} %reshape.57, bf16[32,2,1024,64]{2,3,1,0:T(8,128)(2,1)} %param.23), kind=kOutput, calls=%fused_computation.63 | convolution fusion | flops 8388608 | bytes 8658944 | tf_op jit(solution)/shard_map/bhd,bhpd->bhp/dot_general | solution.py:84
  58.5 2.1 fusion.38
  60.6 1.3 fusion.30
  61.9 5.7 %fusion.11 = f32[32,2,1,64]{3,2,1,0:T(1,128)S(1)} fusion(bf16[32,2,1024,64]{2,3,1,0:T(8,128)(2,1)} %param.24, bf16[32,2,1024,1]{2,1,0,3:T(2,128)(2,1)S(1)} %get-tuple-element.211), kind=kOutput, calls=%fused_computation.24 | convolution fusion | flops 8388608 | bytes 8536064 | tf_op jit(solution)/shard_map/bhp,bhpd->bhd/dot_general | solution.py:92
  67.6 7.5 %all-gather.2 = f32[128,2,64]{2,1,0:T(2,128)S(1)} all-gather(f32[32,2,64]{2,1,0:T(2,128)S(1)} %bitcast.49), channel_id=4, replica_groups=mesh['kv'=4,'tp'=8] {'kv'}, dimensions={0}, use_global_device_ids=true | all-gather | bytes 81920 | tf_op jit(solution)/shard_map/all_gather | solution.py:11
  75.0 0.6 copy-done.3
  75.8 8.1 %all-gather.4 = f32[4,32,2]{1,2,0:T(2,128)S(1)} all-gather(f32[1,32,2]{1,2,0:T(2,128)S(1)} %bitcast.51), channel_id=3, replica_groups=mesh['kv'=4,'tp'=8] {'kv'}, dimensions={0}, use_global_device_ids=true | all-gather | bytes 1280 | tf_op jit(solution)/shard_map/all_gather | solution.py:11
  83.8 7.1 %all-gather.3 = f32[4,32,2]{1,2,0:T(2,128)S(1)} all-gather(f32[1,32,2]{1,2,0:T(2,128)S(1)} %bitcast.50), channel_id=2, replica_groups=mesh['kv'=4,'tp'=8] {'kv'}, dimensions={0}, use_global_device_ids=true | all-gather | bytes 1280 | tf_op jit(solution)/shard_map/all_gather | solution.py:11
  90.9 3.6 %while.19 = (s32[]{:T(128)}, f32[32,2]{0,1:T(2,128)S(1)}, f32[32,2]{0,1:T(2,128)S(1)}, f32[32,2,64]{2,1,0:T(2,128)S(1)}, f32[4,32,2]{1,2,0:T(2,128)S(1)}, /*inde...) while((s32[]{:T(128)}, f32[32,2]{0,1:T(2,128)S(1)}, ...), condition=%wide.region_4.5_spmd, body=%wide.region_3.4_spmd.sunk | while | flops 12677 | bytes 52887 | solution.py:16
  91.1 1.0 fusion.57
  92.3 1.0 fusion.57
  93.5 1.0 fusion.57
  94.6 0.3 fusion.4
  94.9 0.1 reshape.33
  95.0 0.1 multiply_reduce_fusion
  95.2 0.1 copy.36
  95.5 0.3 fusion.3
  95.9 0.2 fusion.22
  96.2 1.8 fusion.42
  98.0 0.7 dynamic_slice.59
  98.7 51.7 %all-reduce.3.cloned.1.call-done = f32[32,1024]{1,0:T(8,128)} async-done(((f32[32,1024]{1,0:T(8,128)}), f32[32,1024]{1,0:T(8,128)}) %all-reduce.3.cloned.1.call-update) | async-done | bytes 131088 | tf_op jit(solution)/shard_map/psum | solution.py:108
  150.4 1.0 fusion.13
  151.4 9.8 %psum.22 = f32[32]{0:T(128)S(1)} all-reduce(f32[32]{0:T(128)S(1)} %get-tuple-element.204), channel_id=1, replica_groups=mesh['kv'=4,'tp'=8] {'kv'}, use_global_device_ids=true, to_apply=%region_8.9 | all-reduce | flops 32 | bytes 256 | tf_op jit(solution)/shard_map/psum | solution.py:113
  161.3 3.8 %fusion.18 = f32[32,2048]{1,0:T(8,128)} fusion(bf16[1024,2048]{1,0:T(8,128)(2,1)} %param.28, bf16[32,1024]{1,0:T(8,128)(2,1)S(1)} %get-tuple-element.205, f32[1024]{0:T(1024)S(1)} %dynamic_slice.59, f32[32]{0:T(128)S(1)} %add_rsqrt_fusion), kind=kOutput, calls=%fused_computation.37 | convolution fusion | flops 134348800 | bytes 4526208 | tf_op jit(solution)/shard_map/dot_general | solution.py:124
  165.1 40.4 %all-reduce.5.cloned.1.call-done = f32[32,2048]{1,0:T(8,128)} async-done(((f32[32,2048]{1,0:T(8,128)}), f32[32,2048]{1,0:T(8,128)}) %all-reduce.5.cloned.1.call-update) | async-done | bytes 262160 | tf_op jit(solution)/shard_map/psum | solution.py:125
  205.5 3.8 %fusion.16 = f32[32,1024]{1,0:T(8,128)} fusion(bf16[2048,1024]{1,0:T(8,128)(2,1)} %param.29, f32[32,2048]{1,0:T(8,128)} %all-reduce.5.cloned.1.call-done), kind=kOutput, calls=%fused_computation.34 | convolution fusion | flops 134414336 | bytes 4587520 | tf_op jit(solution)/shard_map/dot_general | solution.py:126
  209.3 30.7 %reduce-scatter.2.cloned.1.call-done = f32[32,128]{1,0:T(8,128)} async-done(((f32[32,1024]{1,0:T(8,128)}), f32[32,128]{1,0:T(8,128)}) %reduce-scatter.2.cloned.1.call-update) | async-done | bytes 16400 | tf_op jit(solution)/shard_map/reduce_scatter | solution.py:127
  240.0 1.3 add_convert_fusion.1
  (41 shorter events, 1.6 us)
Async XLA Ops:
  6.5 44.8 %copy-start = (bf16[4096,128]{1,0:T(8,128)(2,1)S(1)}, bf16[4096,128]{1,0:T(8,128)(2,1)}, u32[]{:S(2)}) copy-start(bf16[4096,128]{1,0:T(8,128)(2,1)} %param.18) | copy-start | bytes 3145732
  6.5 143.8 %all-reduce.3.cloned.1.call-start = ((), (), s32[]{:S(2)}) async-start(), calls=%async_computation.1 | async-start | bytes 262144 | tf_op jit(solution)/shard_map/psum | solution.py:108
  58.4 36.1 %copy-start.1 = (bf16[4096,128]{1,0:T(8,128)(2,1)S(1)}, bf16[4096,128]{1,0:T(8,128)(2,1)}, u32[]{:S(2)}) copy-start(bf16[4096,128]{1,0:T(8,128)(2,1)} %param.19) | copy-start | bytes 3145732
  58.4 36.1 %copy-start.4 = (f32[4096]{0:T(1024)S(1)}, f32[4096]{0:T(1024)}, u32[]{:S(2)}) copy-start(f32[4096]{0:T(1024)} %param.17) | copy-start | bytes 49156
  58.5 37.0 %copy-start.2 = (bf16[4096,128]{1,0:T(8,128)(2,1)S(1)}, bf16[4096,128]{1,0:T(8,128)(2,1)}, u32[]{:S(2)}) copy-start(bf16[4096,128]{1,0:T(8,128)(2,1)} %param.20) | copy-start | bytes 3145732
  75.0 0.6 copy-start.3
  98.0 107.5 %all-reduce.5.cloned.1.call-start = ((), (), s32[]{:S(2)}) async-start(), calls=%async_computation.2 | async-start | bytes 524288 | tf_op jit(solution)/shard_map/psum | solution.py:125
  165.1 75.0 %reduce-scatter.2.cloned.1.call-start = ((), (), s32[]{:S(2)}) async-start(), calls=%async_computation.3 | async-start | bytes 147456 | tf_op jit(solution)/shard_map/reduce_scatter | solution.py:127
Sparse Core Ops, SparseCore 0:
  98.1 52.2 all-reduce.2
  165.2 40.2 all-reduce.4
  209.4 30.5 reduce-scatter.1
where the time goes:
time: 249 us; the launch traced here: 248 us
  waiting for transfers between devices  123 us (49%)
  blocking collectives  77.1 us (31%)
  matrix products  22.4 us (9%)
  between operations  13.2 us (5%)
  other arithmetic  9.28 us (4%)
  local copies, waits for them, and re-layouts  2.9 us (1%)
    psum x1, waiting for transfers between devices, shards(): block_sum = lax.psum(partial_value, 'tp')  51.7 us
    all_gather x1, blocking collectives, shards(): gathered = lax.all_gather(stream, ('kv', 'tp'), axis=1, tiled=True)  44.6 us
    psum x1, waiting for transfers between devices, shards(): hidden = squared_relu(lax.psum(up_partial, 'kv'))  40.4 us
    reduce_scatter x1, waiting for transfers between devices, shards(): lax.psum_scatter(down_partial, 'tp', scatter_dimension=1, tiled=True)  30.7 us
    all_gather x3, blocking collectives, combined_all(): gathered = jax.tree.map(lambda a: lax.all_gather(a, axis), part)  22.6 us
    psum x1, blocking collectives, shards(): squares = lax.psum(row_squares(middle_block), 'kv')  9.84 us
    dot_general x1, matrix products, shards(): jnp.einsum('bhp,bhpd->bhd', weights, value_cache, preferred_element_type=...  5.65 us
  transfers between devices with their start and end apart: 3, of which 3 were waited for; matrix products, arithmetic and copies ran while one was open for 0% of the time, Pallas kernels for 0%

commit v1 on v0

--- a/solution.py
+++ b/solution.py
@@ -122,7 +122,7 @@
         middle_block.astype(jnp.float32) * inverse[:, None] * gain_block[None, :]
     ).astype(jnp.bfloat16)
     up_partial = jnp.dot(mixed_block, up_weight, preferred_element_type=jnp.float32)
-    hidden = squared_relu(lax.psum(up_partial, "kv"))
+    hidden = squared_relu(jnp.sum(lax.all_gather(up_partial, "kv"), axis=0))
     down_partial = jnp.dot(hidden, down_weight, preferred_element_type=jnp.float32)
     reduced = lax.psum_scatter(down_partial, "tp", scatter_dimension=1, tiled=True)
     return (middle_piece.astype(jnp.float32) + reduced).astype(jnp.bfloat16)

time: 249 us -> 229 us (0.920)
  waiting for transfers between devices: 123 us -> 106 us
  other arithmetic: 9.28 us -> 5.67 us
    psum x1 -> x0, waiting for transfers between devices: 40.4 us -> none  [shards(): hidden = squared_relu(lax.psum(up_partial, 'kv'))]
    all_gather x0 -> x1, waiting for transfers between devices: none -> 23.8 us  [shards(): hidden = squared_relu(jnp.sum(lax.all_gather(up_partial, 'kv'), axis=0))]
where the time goes in v1:
time: 229 us
  waiting for transfers between devices  106 us (46%)
  blocking collectives  77.1 us (34%)
  matrix products  23.9 us (10%)
  between operations  13.2 us (6%)
  other arithmetic  5.67 us (2%)
    psum x1, waiting for transfers between devices, shards(): block_sum = lax.psum(partial_value, 'tp')  51.6 us
    all_gather x1, blocking collectives, shards(): gathered = lax.all_gather(stream, ('kv', 'tp'), axis=1, tiled=True)  44.6 us
    reduce_scatter x1, waiting for transfers between devices, shards(): lax.psum_scatter(down_partial, 'tp', scatter_dimension=1, tiled=True)  30.7 us
    all_gather x1, waiting for transfers between devices, shards(): hidden = squared_relu(jnp.sum(lax.all_gather(up_partial, 'kv'), axis=0))  23.8 us
    all_gather x3, blocking collectives, combined_all(): gathered = jax.tree.map(lambda a: lax.all_gather(a, axis), part)  22.6 us
    psum x1, blocking collectives, shards(): squares = lax.psum(row_squares(middle_block), 'kv')  9.84 us
    dot_general x1, matrix products, shards(): jnp.einsum('bhp,bhpd->bhd', weights, value_cache, preferred_element_type=...  5.64 us
  transfers between devices with their start and end apart: 3, of which 3 were waited for; matrix products, arithmetic and copies ran while one was open for 0% of the time, Pallas kernels for 0%

profile of v1, /device:TPU:0, one launch (start us, length us, event | category | flops | bytes accessed | tf_op | source)
XLA Modules:
  0.0 228.5 jit_solution(15414133980276026750)
XLA Ops:
  6.5 44.6 %all_gather.27 = bf16[32,4096]{1,0:T(8,128)(2,1)S(1)} all-gather(bf16[32,128]{1,0:T(8,128)(2,1)} %param.16), channel_id=1, replica_groups=mesh['kv'=4,'tp'=8] {'kv','tp'}, dimensions={1}, use_global_device_ids=true | all-gather | bytes 270336 | tf_op jit(solution)/shard_map/all_gather | solution.py:69
  51.2 0.2 fusion.6
  51.4 1.0 convolution_convert_fusion.2
  52.6 1.6 fusion.4
  54.2 0.1 reshape.33
  54.3 0.1 multiply_reduce_fusion
  54.5 1.6 fusion.3
  56.1 1.2 fusion.40
  57.4 0.1 reshape.34
  57.5 4.6 %fusion.41 = f32[32,2,1,1024]{3,2,1,0:T(1,128)S(1)} fusion(bf16[32,2,64,1]{2,3,1,0:T(2,128)(2,1)S(1)} %reshape.58, bf16[32,2,1024,64]{2,3,1,0:T(8,128)(2,1)} %param.23), kind=kOutput, calls=%fused_computation.63 | convolution fusion | flops 8388608 | bytes 8658944 | tf_op jit(solution)/shard_map/bhd,bhpd->bhp/dot_general | solution.py:84
  62.0 0.4 fusion.38
  62.5 0.4 fusion.30
  62.9 7.1 %all-gather.5 = f32[4,32,2]{1,2,0:T(2,128)S(1)} all-gather(f32[1,32,2]{1,2,0:T(2,128)S(1)} %bitcast.53), channel_id=3, replica_groups=mesh['kv'=4,'tp'=8] {'kv'}, dimensions={0}, use_global_device_ids=true | all-gather | bytes 1280 | tf_op jit(solution)/shard_map/all_gather | solution.py:11
  70.0 8.1 %all-gather.4 = f32[4,32,2]{1,2,0:T(2,128)S(1)} all-gather(f32[1,32,2]{1,2,0:T(2,128)S(1)} %bitcast.52), channel_id=2, replica_groups=mesh['kv'=4,'tp'=8] {'kv'}, dimensions={0}, use_global_device_ids=true | all-gather | bytes 1280 | tf_op jit(solution)/shard_map/all_gather | solution.py:11
  78.1 5.6 %fusion.11 = f32[32,2,1,64]{3,2,1,0:T(1,128)S(1)} fusion(bf16[32,2,1024,64]{2,3,1,0:T(8,128)(2,1)} %param.24, bf16[32,2,1024,1]{2,1,0,3:T(2,128)(2,1)S(1)} %get-tuple-element.211), kind=kOutput, calls=%fused_computation.24 | convolution fusion | flops 8388608 | bytes 8536064 | tf_op jit(solution)/shard_map/bhp,bhpd->bhd/dot_general | solution.py:92
  83.7 7.5 %all-gather.2 = f32[128,2,64]{2,1,0:T(2,128)S(1)} all-gather(f32[32,2,64]{2,1,0:T(2,128)S(1)} %bitcast.51), channel_id=4, replica_groups=mesh['kv'=4,'tp'=8] {'kv'}, dimensions={0}, use_global_device_ids=true | all-gather | bytes 81920 | tf_op jit(solution)/shard_map/all_gather | solution.py:11
  91.2 1.4 while.19
  91.4 0.2 fusion.57
  91.9 0.2 fusion.57
  92.3 0.2 fusion.57
  92.9 0.2 fusion.22
  93.1 0.8 fusion.42
  94.0 0.7 dynamic_slice.59
  94.7 51.6 %all-reduce.2.cloned.1.call-done = f32[32,1024]{1,0:T(8,128)} async-done(((f32[32,1024]{1,0:T(8,128)}), f32[32,1024]{1,0:T(8,128)}) %all-reduce.2.cloned.1.call-update) | async-done | bytes 131088 | tf_op jit(solution)/shard_map/psum | solution.py:108
  146.4 1.0 fusion.13
  147.4 9.8 %psum.15 = f32[32]{0:T(128)S(1)} all-reduce(f32[32]{0:T(128)S(1)} %get-tuple-element.204), channel_id=1, replica_groups=mesh['kv'=4,'tp'=8] {'kv'}, use_global_device_ids=true, to_apply=%region_8.9 | all-reduce | flops 32 | bytes 256 | tf_op jit(solution)/shard_map/psum | solution.py:113
  157.2 3.8 %fusion.18 = f32[32,2048]{1,0:T(8,128)} fusion(bf16[1024,2048]{1,0:T(8,128)(2,1)} %param.28, bf16[32,1024]{1,0:T(8,128)(2,1)S(1)} %get-tuple-element.205, f32[1024]{0:T(1024)S(1)} %dynamic_slice.59, f32[32]{0:T(128)S(1)} %add_rsqrt_fusion), kind=kOutput, calls=%fused_computation.37 | convolution fusion | flops 134348800 | bytes 4526208 | tf_op jit(solution)/shard_map/dot_general | solution.py:124
  161.1 23.8 %all-gather.8.cloned.1.call-done = f32[128,2048]{1,0:T(8,128)} async-done(((f32[32,2048]{1,0:T(8,128)}), f32[128,2048]{1,0:T(8,128)}) %all-gather.8.cloned.1.call-update) | async-done | bytes 1048592 | tf_op jit(solution)/shard_map/all_gather | solution.py:125
  184.9 1.3 reduce_sum.49
  186.3 3.7 %fusion.16 = f32[32,1024]{1,0:T(8,128)} fusion(bf16[2048,1024]{1,0:T(8,128)(2,1)} %param.29, f32[32,2048]{1,0:T(8,128)S(1)} %reduce_sum.49), kind=kOutput, calls=%fused_computation.34 | convolution fusion | flops 134414336 | bytes 4587520 | tf_op jit(solution)/shard_map/dot_general | solution.py:126
  189.9 30.7 %reduce-scatter.2.cloned.1.call-done = f32[32,128]{1,0:T(8,128)} async-done(((f32[32,1024]{1,0:T(8,128)}), f32[32,128]{1,0:T(8,128)}) %reduce-scatter.2.cloned.1.call-update) | async-done | bytes 16400 | tf_op jit(solution)/shard_map/reduce_scatter | solution.py:127
  220.7 1.3 add_convert_fusion.1
  (38 shorter events, 1.6 us)
Async XLA Ops:
  6.5 44.8 %copy-start = (bf16[4096,128]{1,0:T(8,128)(2,1)S(1)}, bf16[4096,128]{1,0:T(8,128)(2,1)}, u32[]{:S(2)}) copy-start(bf16[4096,128]{1,0:T(8,128)(2,1)} %param.18) | copy-start | bytes 3145732
  6.5 139.8 %all-reduce.2.cloned.1.call-start = ((), (), s32[]{:S(2)}) async-start(), calls=%async_computation.1 | async-start | bytes 262144 | tf_op jit(solution)/shard_map/psum | solution.py:108
  54.4 7.6 %copy-start.1 = (f32[32,2,1024]{2,1,0:T(2,128)S(1)}, f32[32,2,1024]{2,1,0:T(2,128)}, u32[]{:S(2)}) copy-start(f32[32,2,1024]{2,1,0:T(2,128)} %param.25) | copy-start | bytes 786436
  62.0 31.1 %copy-start.2 = (bf16[128,1024]{1,0:T(8,128)(2,1)S(1)}, bf16[128,1024]{1,0:T(8,128)(2,1)}, u32[]{:S(2)}) copy-start(bf16[128,1024]{1,0:T(8,128)(2,1)} %param.26) | copy-start | bytes 786436
  94.0 91.0 %all-gather.8.cloned.1.call-start = ((), (), s32[]{:S(2)}) async-start(), calls=%async_computation.3 | async-start | bytes 1310720 | tf_op jit(solution)/shard_map/all_gather | solution.py:125
  161.1 59.6 %reduce-scatter.2.cloned.1.call-start = ((), (), s32[]{:S(2)}) async-start(), calls=%async_computation.2 | async-start | bytes 147456 | tf_op jit(solution)/shard_map/reduce_scatter | solution.py:127
Sparse Core Ops, SparseCore 0:
  94.1 52.2 all-reduce.1
  161.2 23.7 all-gather.7
  190.1 30.5 reduce-scatter.1
